TPU v7x, 256 devices: a whole 4x4x8 slice. The times are simulated.
256 devices in a mesh: ep: 64 (over z, x, core), tp: 4 (over y).
Axes of the slice: x: 4, y: 4, z: 8, core: 2. Of those that a mesh axis runs over, the one named last changes fastest.
Arguments:
- pool_input: bfloat16 [32768, 1024], P('ep', 'tp'), may hold values from -6 to 6
- group_weight: bfloat16 [4, 256, 256], P('tp'), may hold values from -0.375 to 0.375
- pool_scale: float32 [1024], P('tp'), may hold values from 0.1 to 1.9
- out_weight: bfloat16 [1024, 2048], P('tp'), may hold values from -0.1875 to 0.1875
- mix_gain: float32 [2048], replicated, may hold values from 0.1 to 1.9
- expert_input: bfloat16 [65536, 2048], P(('ep', 'tp')), may hold values from -6 to 6
- routes: int32 [65536, 2], P('ep'), may hold values from 0 to 127, all different within a row; in each aligned block of 256 rows (0 to 255, 256 to 511, ...) at most 5 rows name the same one
- route_weights: float32 [65536, 2], P('ep'), may hold values from 0.2 to 2.5
- moe_in_gain: float32 [2048], replicated, may hold values from 0.1 to 1.9
- gate_weight: bfloat16 [128, 2048, 1024], P('ep', None, 'tp'), may hold values from -0.125 to 0.125
- up_weight: bfloat16 [128, 2048, 1024], P('ep', None, 'tp'), may hold values from -0.125 to 0.125
- down_weight: bfloat16 [128, 1024, 2048], P('ep', 'tp'), may hold values from -0.1875 to 0.1875
- moe_out_gain: float32 [2048], replicated, may hold values from 0.1 to 1.9
Outputs:
- mixer_out: bfloat16 [32768, 2048], P(('ep', 'tp'))
- moe_out: bfloat16 [65536, 2048], P(('ep', 'tp'))
Inputs may be any that keep to these rules, and one draw needn't show every extreme that they name: `routes`: each row names 2 different experts. In each aligned block of 256 rows no expert is named by more than 5 rows, a bound that some block reaches.
All inputs are finite; a program needn't handle non-finite values.
Results may differ from a plain program's by a relative error of at most 0.013.
Values may be sent and summed in bfloat16 or wider, within the bound.
No kernel may reach another device: no remote copies, remote signals or barrier semaphores. Data moves between devices by JAX's collectives and lax.ppermute only.
A program may use at most 128 MiB of HBM per device.

v0:
```python
import jax
import jax.numpy as jnp
from jax import lax
from jax.sharding import PartitionSpec as P

NORM_EPS = 1e-06


def passed_along(value, axis, steps):
    count = lax.axis_size(axis)
    initial, last = (max(0, -steps), min(count, count - steps))
    return lax.ppermute(value, axis, [(source, source + steps) for source in range(initial, last)])


def rms_scale(values, gain_vec):
    mean_sq = jnp.mean(values * values, axis=-1, keepdims=True)
    return values * lax.rsqrt(mean_sq + NORM_EPS) * gain_vec


def slot_numbers(route_block, experts, capacity):
    flat_routes = route_block.reshape(-1)
    one_hot = (flat_routes[:, None] == jnp.arange(experts, dtype=jnp.int32)[None, :]).astype(
        jnp.int32
    )
    slot_rank = jnp.sum((jnp.cumsum(one_hot, axis=0) - one_hot) * one_hot, axis=1)
    return flat_routes * capacity + slot_rank


def fill_table(slot_ids, payload, empty_value, slots_total):
    return jnp.full((slots_total,), empty_value, payload.dtype).at[slot_ids].set(payload)


def on_device(
    pool_input,
    group_weight,
    pool_scale,
    out_weight,
    mix_gain,
    expert_input,
    routes,
    route_weights,
    moe_in_gain,
    gate_weight,
    up_weight,
    down_weight,
    moe_out_gain,
):
    tp_size = lax.axis_size("tp")
    ep_size = lax.axis_size("ep")
    tp_index = lax.axis_index("tp")
    rows_a = pool_input.shape[0]
    model_width = out_weight.shape[1]
    history_rows = 2**tp_size
    window = jnp.left_shift(jnp.int32(2), tp_index)
    history = passed_along(pool_input[rows_a - history_rows :], "ep", 1)
    extended = jnp.concatenate([history, pool_input], axis=0).astype(jnp.float32)
    running = jnp.cumsum(extended, axis=0)
    lagged = lax.dynamic_slice_in_dim(running, history_rows - window, rows_a, 0)
    current = running[history_rows:]
    position = lax.axis_index("ep") * rows_a + jnp.arange(rows_a, dtype=jnp.int32)
    divisor = jnp.minimum(position + 1, window).astype(jnp.float32)[:, None]
    pooled = ((current - lagged) / divisor - extended[history_rows:]).astype(jnp.bfloat16)
    grouped = (
        jnp.dot(pooled, group_weight[0], preferred_element_type=jnp.float32) * pool_scale
    ).astype(jnp.bfloat16)
    exp_dev = gate_weight.shape[0]
    experts = exp_dev * ep_size
    tok_dev = expert_input.shape[0]
    top_count = routes.shape[1]
    capacity = max(2, 5 * tok_dev * top_count // (4 * experts))
    slots_total = experts * capacity
    normed = rms_scale(expert_input.astype(jnp.float32), moe_in_gain).astype(jnp.bfloat16)
    own_routes = lax.dynamic_slice_in_dim(routes, tp_index * tok_dev, tok_dev, 0)
    own_slots = slot_numbers(own_routes, experts, capacity)
    pair_token = jnp.arange(tok_dev * top_count, dtype=jnp.int32) // top_count
    token_table = fill_table(own_slots, pair_token, tok_dev, slots_total)
    padded_rows = jnp.concatenate([normed, jnp.zeros((1, model_width), jnp.bfloat16)], axis=0)
    outgoing = padded_rows[token_table].reshape(ep_size, exp_dev * capacity, model_width)
    arrived = lax.all_to_all(outgoing, "ep", split_axis=0, concat_axis=0, tiled=True)
    received = lax.all_gather(arrived[None], "tp", axis=0, tiled=True)
    per_quarter = ep_size * exp_dev * capacity
    flat_in = received.reshape(tp_size * per_quarter, model_width)
    projected = lax.psum_scatter(
        jnp.dot(grouped, out_weight, preferred_element_type=jnp.float32).astype(jnp.bfloat16),
        "tp",
        scatter_dimension=0,
        tiled=True,
    ).astype(jnp.float32)
    piece_rows = flat_in
    piece_rows = piece_rows.reshape(
        per_quarter * lax.axis_size("tp") // (exp_dev * capacity), exp_dev, capacity, model_width
    )
    gate_act = jnp.einsum(
        "nxcd,xdf->nxcf", piece_rows, gate_weight, preferred_element_type=jnp.float32
    )
    up_act = jnp.einsum("nxcd,xdf->nxcf", piece_rows, up_weight, preferred_element_type=jnp.float32)
    hidden = (jax.nn.silu(gate_act) * up_act).astype(jnp.bfloat16)
    down_act = jnp.einsum("nxcf,xfd->nxcd", hidden, down_weight, preferred_element_type=jnp.float32)
    expert_sum = lax.psum_scatter(
        down_act.reshape(per_quarter * lax.axis_size("tp"), model_width).astype(jnp.bfloat16),
        "tp",
        scatter_dimension=0,
        tiled=True,
    )
    mixer_out = rms_scale(projected, mix_gain).astype(jnp.bfloat16)
    expert_back = expert_sum.reshape(ep_size, exp_dev * capacity, model_width)
    returned = lax.all_to_all(expert_back, "ep", split_axis=0, concat_axis=0, tiled=True)
    picked = returned.reshape(slots_total, model_width)[own_slots].reshape(
        tok_dev, top_count, model_width
    )
    own_weights = lax.dynamic_slice_in_dim(route_weights, tp_index * tok_dev, tok_dev, 0)
    combined = jnp.sum(picked.astype(jnp.float32) * own_weights[:, :, None], axis=1)
    moe_out = rms_scale(combined, moe_out_gain).astype(jnp.bfloat16)
    return (mixer_out, moe_out)


def solution(mesh):
    in_specs = (
        P("ep", "tp"),
        P("tp", None, None),
        P("tp"),
        P("tp", None),
        P(),
        P(("ep", "tp"), None),
        P("ep", None),
        P("ep", None),
        P(),
        P("ep", None, "tp"),
        P("ep", None, "tp"),
        P("ep", "tp", None),
        P(),
    )
    out_specs = (P(("ep", "tp"), None), P(("ep", "tp"), None))
    return jax.shard_map(
        on_device, mesh=mesh, in_specs=in_specs, out_specs=out_specs, check_vma=False
    )
```

profile of v0, /device:TPU:2, one launch (start us, length us, event | category | flops | bytes accessed | tf_op | source)
XLA Modules:
  0.0 536.5 jit_solution(6434303387397360393)
XLA Ops:
  7.2 0.0 copy-start
  7.2 0.0 copy-start.2
  7.2 0.0 copy-start.6
  7.2 0.0 all-gather.3.cloned.1.call-start
  7.3 0.8 broadcast_multiply_fusion
  8.1 0.1 copy.31
  8.2 0.1 eq.29
  8.4 0.1 eq.25
  8.5 0.6 add_select_fusion
  9.1 0.1 copy.33
  9.2 0.2 fusion.29
  9.5 0.1 copy.30
  9.7 0.1 mul.122
  9.8 0.2 fusion.28
  10.1 2.6 scatter_custom_fusion
  12.7 0.0 copy-done.2
  12.7 0.3 fusion.4
  13.0 0.0 copy-done.6
  13.0 0.3 fusion.6
  13.3 0.1 concatenate.7
  13.4 4.1 gather_fusion
  17.5 5.4 %reshape.113 = bf16[64,10,2048]{2,1,0:T(8,128)(2,1)} reshape(bf16[640,2048]{1,0:T(8,128)(2,1)} %gather_fusion) | data formatting | bytes 5242880 | tf_op jit(solution)/shard_map/reshape | solution.py:78
  22.9 108.2 %all_to_all.10 = bf16[64,10,2048]{2,1,0:T(8,128)(2,1)S(1)} all-to-all(bf16[64,10,2048]{2,1,0:T(8,128)(2,1)} %reshape.113), channel_id=1, replica_groups=mesh['ep'=64,'tp'=4] {'ep'}, dimensions={0} | all-to-all | bytes 5242880 | tf_op jit(solution)/shard_map/all_to_all | solution.py:79
  131.1 3.0 copy.35
  134.0 0.0 all-gather.3.cloned.1.call-update
  134.1 0.2 reduce-scatter.5.cloned.1.call-start
  134.3 99.6 %all-gather.3.cloned.1.call-done = bf16[256,10,2048]{2,0,1:T(8,128)(2,1)} async-done(((bf16[64,10,2048]{2,0,1:T(8,128)(2,1)}), bf16[256,10,2048]{2,0,1:T(8,128)(2,1)}) %all-gather.3.cloned.1.call-update) | async-done | bytes 10485776 | tf_op jit(solution)/shard_map/all_gather | solution.py:80
  233.9 9.0 %fusion.14 = f32[2,256,5,256]{3,1,2,0:T(8,128)} fusion(bf16[256,2,5,2048]{3,0,2,1:T(8,128)(2,1)} %bitcast.84, bf16[2,2048,256]{2,1,0:T(8,128)(2,1)} %param.22), kind=kOutput, calls=%fused_computation.21 | convolution fusion | flops 2684354560 | bytes 15204352 | tf_op jit(solution)/shard_map/nxcd,xdf->nxcf/dot_general | solution.py:93
  242.9 0.0 copy-done
  242.9 16.3 %convert_bitcast_fusion = bf16[256,2,5,2048]{3,0,2,1:T(8,128)(2,1)} fusion(bf16[2,256,2048]{2,1,0:T(8,128)(2,1)S(1)} %copy-done, f32[2,256,5,256]{3,1,2,0:T(8,128)} %fusion.14, bf16[256,2,5,2048]{3,0,2,1:T(8,128)(2,1)} %bitcast.85, bf16[2,2048,256]{2,1,0:T(8,128)(2,1)} %param.23), kind=kOutput, calls=%fused_computation.3 | convolution fusion | flops 5377884160 | bytes 27787264 | tf_op jit(solution)/shard_map/nxcf,xfd->nxcd/dot_general | solution.py:98
  259.2 15.3 %copy.36 = bf16[256,2,5,2048]{3,2,1,0:T(8,128)(2,1)} copy(bf16[256,2,5,2048]{3,0,2,1:T(8,128)(2,1)} %convert_bitcast_fusion) | data formatting | bytes 20971520 | tf_op jit(solution)/shard_map/convert_element_type | solution.py:100
  274.5 18.4 %convert_element_type.73 = bf16[2560,2048]{1,0:T(8,128)(2,1)} reshape(bf16[256,2,5,2048]{3,2,1,0:T(8,128)(2,1)} %copy.36) | data formatting | bytes 20971520 | tf_op jit(solution)/shard_map/convert_element_type | solution.py:100
  293.0 0.0 reduce-scatter.5.cloned.1.call-update
  293.0 0.9 copy-done.4
  293.9 1.9 collective-permute-start
  295.9 3.0 collective-permute-done
  298.9 0.1 fusion.37
  299.0 0.7 fusion.21
  299.7 0.1 broadcast_add_fusion
  299.8 0.2 copy.29
  300.0 94.2 %reduce-scatter.5.cloned.1.call-done = bf16[640,2048]{1,0:T(8,128)(2,1)} async-done(((bf16[2560,2048]{1,0:T(8,128)(2,1)}), bf16[640,2048]{1,0:T(8,128)(2,1)}) %reduce-scatter.5.cloned.1.call-update) | async-done | bytes 2621456 | tf_op jit(solution)/shard_map/reduce_scatter | solution.py:99
  394.2 5.4 %reshape.114 = bf16[64,10,2048]{2,1,0:T(8,128)(2,1)} reshape(bf16[640,2048]{1,0:T(8,128)(2,1)} %reduce-scatter.5.cloned.1.call-done) | data formatting | bytes 5242880 | tf_op jit(solution)/shard_map/reshape | solution.py:106
  399.6 10.9 %all-to-all-start.1 = ((bf16[64,10,2048]{2,1,0:T(8,128)(2,1)}), bf16[64,10,2048]{2,1,0:T(8,128)(2,1)}, u32[]{:S(2)}, u32[]{:S(2)}) async-start(bf16[64,10,2048]{2,1,0:T(8,128)(2,1)} %reshape.114), calls=%async_computation.3 | async-start | bytes 8388608 | tf_op jit(solution)/shard_map/all_to_all | solution.py:107
  410.5 0.3 reduce-scatter.3.cloned.1.call-start
  410.8 0.0 copy-done.3
  410.8 0.0 copy-done.5
  410.8 0.0 copy-done.9
  410.8 0.0 copy-start.7
  410.8 2.3 convolution_convert_fusion
  413.1 0.0 reduce-scatter.3.cloned.1.call-update
  413.1 0.7 constant_dynamic-slice_fusion
  413.8 0.1 copy.37
  414.0 31.7 %reduce-scatter.3.cloned.1.call-done = bf16[128,2048]{1,0:T(8,128)(2,1)} async-done(((bf16[512,2048]{1,0:T(8,128)(2,1)}), bf16[128,2048]{1,0:T(8,128)(2,1)}) %reduce-scatter.3.cloned.1.call-update) | async-done | bytes 524304 | tf_op jit(solution)/shard_map/reduce_scatter | solution.py:83
  445.6 1.2 fusion.18
  446.9 0.0 copy-done.7
  446.9 2.0 fusion.20
  448.9 57.7 %all-to-all-done.1 = bf16[64,10,2048]{2,1,0:T(8,128)(2,1)} async-done(((bf16[64,10,2048]{2,1,0:T(8,128)(2,1)}), bf16[64,10,2048]{2,1,0:T(8,128)(2,1)}, u32[]{:S(2)}, u32[]{:S(2)}) %all-to-all-start.1) | async-done | bytes 2621472 | tf_op jit(solution)/shard_map/all_to_all | solution.py:107
  506.6 4.1 reshape.115
  510.7 3.3 gather_fusion.1
  514.0 5.4 %reshape.116 = f32[256,2,2048]{2,1,0:T(2,128)} reshape(bf16[512,2048]{1,0:T(8,128)(2,1)} %gather_fusion.1) | data formatting | bytes 6291456 | tf_op jit(solution)/shard_map/convert_element_type | solution.py:112
  519.5 9.0 %multiply_reduce_fusion = f32[256,2048]{1,0:T(8,128)S(1)} fusion(f32[256,2,2048]{2,1,0:T(2,128)} %reshape.116, f32[256,2]{1,0:T(8,128)S(1)} %copy.37), kind=kLoop, calls=%fused_computation.4 | loop fusion | flops 1572864 | bytes 6293504 | tf_op jit(solution)/shard_map/reduce_sum | solution.py:112
  528.5 0.2 multiply_reduce_fusion.1
  528.7 0.0 copy-done.8
  528.7 1.2 multiply_convert_fusion
  (26 shorter events, 0.3 us)
Async XLA Ops:
  7.2 235.7 %copy-start = (bf16[2,256,2048]{2,1,0:T(8,128)(2,1)S(1)}, bf16[2,256,2048]{2,1,0:T(8,128)(2,1)}, u32[]{:S(2)}) copy-start(bf16[2,256,2048]{2,1,0:T(8,128)(2,1)} %param.24) | copy-start | bytes 6291460
  7.2 5.5 %copy-start.2 = (bf16[256,2048]{1,0:T(8,128)(2,1)S(1)}, bf16[256,2048]{1,0:T(8,128)(2,1)}, u32[]{:S(2)}) copy-start(bf16[256,2048]{1,0:T(8,128)(2,1)} %param.18) | copy-start | bytes 3145732
  7.2 5.8 %copy-start.6 = (f32[2048]{0:T(1024)S(1)}, f32[2048]{0:T(1024)}, u32[]{:S(2)}) copy-start(f32[2048]{0:T(1024)} %param.21) | copy-start | bytes 24580
  7.2 226.7 %all-gather.3.cloned.1.call-start = ((), (), s32[]{:S(2)}) async-start(), calls=%async_computation.6 | async-start | bytes 13107200 | tf_op jit(solution)/shard_map/all_gather | solution.py:80
  134.1 260.2 %reduce-scatter.5.cloned.1.call-start = ((), (), s32[]{:S(2)}) async-start(), calls=%async_computation.5 | async-start | bytes 13107200 | tf_op jit(solution)/shard_map/reduce_scatter | solution.py:99
  293.0 0.9 copy-start.4
  293.9 5.0 collective-permute-start
  399.6 11.2 %copy-start.3 = (bf16[256,2048]{1,0:T(8,128)(2,1)S(1)}, bf16[256,2048]{1,0:T(8,128)(2,1)}, u32[]{:S(2)}) copy-start(bf16[256,2048]{1,0:T(8,128)(2,1)} %param.16) | copy-start | bytes 3145732
  399.6 11.2 %copy-start.5 = (bf16[1,256,256]{2,1,0:T(8,128)(2,1)S(1)}, bf16[1,256,256]{2,1,0:T(8,128)(2,1)}, u32[]{:S(2)}) copy-start(bf16[1,256,256]{2,1,0:T(8,128)(2,1)} %param.14) | copy-start | bytes 393220
  399.6 11.2 %copy-start.9 = (f32[256]{0:T(256)S(1)}, f32[256]{0:T(256)}, u32[]{:S(2)}) copy-start(f32[256]{0:T(256)} %param.15) | copy-start | bytes 3076
  399.6 107.0 %all-to-all-start.1 = ((bf16[64,10,2048]{2,1,0:T(8,128)(2,1)}), bf16[64,10,2048]{2,1,0:T(8,128)(2,1)}, u32[]{:S(2)}, u32[]{:S(2)}) async-start(bf16[64,10,2048]{2,1,0:T(8,128)(2,1)} %reshape.114), calls=%async_computation.3 | async-start | bytes 8388608 | tf_op jit(solution)/shard_map/all_to_all | solution.py:107
  410.5 35.1 %reduce-scatter.3.cloned.1.call-start = ((), (), s32[]{:S(2)}) async-start(), calls=%async_computation.4 | async-start | bytes 2621440 | tf_op jit(solution)/shard_map/reduce_scatter | solution.py:83
  410.8 36.1 %copy-start.7 = (f32[2048]{0:T(1024)S(1)}, f32[2048]{0:T(1024)}, u32[]{:S(2)}) copy-start(f32[2048]{0:T(1024)} %param.17) | copy-start | bytes 24580
  519.4 9.3 %copy-start.8 = (f32[2048]{0:T(1024)S(1)}, f32[2048]{0:T(1024)}, u32[]{:S(2)}) copy-start(f32[2048]{0:T(1024)} %param.25) | copy-start | bytes 24580
  519.4 10.5 %copy-start.1 = (bf16[2,256,2048]{2,1,0:T(8,128)(2,1)S(1)}, bf16[2,256,2048]{2,1,0:T(8,128)(2,1)}, u32[]{:S(2)}) copy-start(bf16[2,256,2048]{2,1,0:T(8,128)(2,1)} %param.24) | copy-start | bytes 6291460
Sparse Core Ops, SparseCore 0:
  134.2 99.7 all-gather.2
  293.1 101.0 reduce-scatter.4
  413.9 31.7 reduce-scatter.2
where the time goes:
time: 538 us; the launch traced here: 536 us
  waiting for transfers between devices  286 us (53%)
  blocking collectives  108 us (20%)
  local copies, waits for them, and re-layouts  70 us (13%)
  matrix products  27.6 us (5%)
  other arithmetic  17.1 us (3%)
  between operations  14.1 us (3%)
  starting transfers between devices  13.3 us (2%)
    all_to_all x1, blocking collectives, on_device(): lax.all_to_all(outgoing, 'ep', split_axis=0, concat_axis=0, tiled=True)  108 us
    all_gather x1, waiting for transfers between devices, on_device(): received = lax.all_gather(arrived[None], 'tp', axis=0, tiled=True)  99.6 us
    reduce_scatter x1, waiting for transfers between devices, on_device(): lax.psum_scatter(down_act.reshape(per_quarter * lax.axis_size('tp'), mode...  94.2 us
    all_to_all x1, waiting for transfers between devices, on_device(): lax.all_to_all(expert_back, 'ep', split_axis=0, concat_axis=0, tiled=True)  57.7 us
    convert_element_type x2, local copies, waits for them, and re-layouts, on_device(): down_act.reshape(per_quarter * lax.axis_size('tp'), model_width)  33.8 us
    reduce_scatter x1, waiting for transfers between devices, on_device(): lax.psum_scatter(jnp.dot(grouped, out_weight, preferred_element_type=jnp....  31.7 us
    dot_general x1, matrix products, on_device(): jnp.einsum('nxcf,xfd->nxcd', hidden, down_weight, preferred_element_type=...  16.3 us
    all_to_all x1, starting transfers between devices, on_device(): lax.all_to_all(expert_back, 'ep', split_axis=0, concat_axis=0, tiled=True)  10.9 us
  transfers between devices with their start and end apart: 5, of which 5 were waited for; matrix products, arithmetic and copies ran while one was open for 1% of the time, Pallas kernels for 0%

commit v1 on v0

--- a/solution.py
+++ b/solution.py
@@ -4,6 +4,24 @@
 from jax.sharding import PartitionSpec as P
 
 NORM_EPS = 1e-06
+
+
+def ring_gather(shard, axis, dim):
+    ways, here, hop = (lax.axis_size(axis), lax.axis_index(axis), shard.shape[dim])
+    shape = [n * ways if d == dim else n for d, n in enumerate(shard.shape)]
+    full = lax.dynamic_update_slice_in_dim(
+        jnp.zeros(shape, shard.dtype), shard, here * hop, axis=dim
+    )
+    going_up = going_down = shard
+    for far in range(1, ways // 2 + 1):
+        going_up = lax.ppermute(going_up, axis, [(d, (d + 1) % ways) for d in range(ways)])
+        full = lax.dynamic_update_slice_in_dim(full, going_up, (here - far) % ways * hop, axis=dim)
+        if 2 * far < ways:
+            going_down = lax.ppermute(going_down, axis, [(d, (d - 1) % ways) for d in range(ways)])
+            full = lax.dynamic_update_slice_in_dim(
+                full, going_down, (here + far) % ways * hop, axis=dim
+            )
+    return full
 
 
 def passed_along(value, axis, steps):
@@ -77,7 +95,7 @@
     padded_rows = jnp.concatenate([normed, jnp.zeros((1, model_width), jnp.bfloat16)], axis=0)
     outgoing = padded_rows[token_table].reshape(ep_size, exp_dev * capacity, model_width)
     arrived = lax.all_to_all(outgoing, "ep", split_axis=0, concat_axis=0, tiled=True)
-    received = lax.all_gather(arrived[None], "tp", axis=0, tiled=True)
+    received = ring_gather(arrived[None], "tp", 0)
     per_quarter = ep_size * exp_dev * capacity
     flat_in = received.reshape(tp_size * per_quarter, model_width)
     projected = lax.psum_scatter(

time: 538 us -> 555 us (1.032)
  local copies, waits for them, and re-layouts: 70 us -> 89 us
    all_gather x1 -> x0, waiting for transfers between devices: 99.6 us -> none  [on_device(): received = lax.all_gather(arrived[None], 'tp', axis=0, tiled=True)]
    ppermute x0 -> x3, waiting for transfers between devices: none -> 97.6 us  [the longest x2 97.6 us: ring_gather(): lax.ppermute(going_up, axis, [(d, (d + 1) % ways) for d in range(ways)])]
    dynamic_update_slice x0 -> x4, local copies, waits for them, and re-layouts: none -> 13.6 us  [the longest x2 7.15 us: ring_gather(): lax.dynamic_update_slice_in_dim(full, going_up, (here - far) % ways * hop...]
    broadcast_in_dim x0 -> x2, local copies, waits for them, and re-layouts: none -> 8.29 us  [the longest x1 5.32 us: ring_gather(): jnp.zeros(shape, shard.dtype)]
  transfers between devices with their start and end apart: 5 -> 7, of which waited for: 5 -> 6; matrix products, arithmetic and copies ran while one was open for 1% -> 4% of each run, Pallas kernels for 0% -> 0%
where the time goes in v1:
time: 555 us; the launch traced here: 553 us
  waiting for transfers between devices  281 us (51%)
  blocking collectives  108 us (19%)
  local copies, waits for them, and re-layouts  89 us (16%)
  matrix products  27 us (5%)
  other arithmetic  17.1 us (3%)
  starting transfers between devices  16.6 us (3%)
  between operations  14.4 us (3%)
    all_to_all x1, blocking collectives, on_device(): lax.all_to_all(outgoing, 'ep', split_axis=0, concat_axis=0, tiled=True)  108 us
    ppermute x2, waiting for transfers between devices, ring_gather(): lax.ppermute(going_up, axis, [(d, (d + 1) % ways) for d in range(ways)])  97.6 us
    reduce_scatter x1, waiting for transfers between devices, on_device(): lax.psum_scatter(down_act.reshape(per_quarter * lax.axis_size('tp'), mode...  90.7 us
    all_to_all x1, waiting for transfers between devices, on_device(): lax.all_to_all(expert_back, 'ep', split_axis=0, concat_axis=0, tiled=True)  57.7 us
    convert_element_type x2, local copies, waits for them, and re-layouts, on_device(): down_act.reshape(per_quarter * lax.axis_size('tp'), model_width)  33.8 us
    reduce_scatter x1, waiting for transfers between devices, on_device(): lax.psum_scatter(jnp.dot(grouped, out_weight, preferred_element_type=jnp....  31.9 us
    dot_general x1, matrix products, on_device(): jnp.einsum('nxcf,xfd->nxcd', hidden, down_weight, preferred_element_type=...  16.3 us
  transfers between devices with their start and end apart: 7, of which 6 were waited for; matrix products, arithmetic and copies ran while one was open for 4% of the time, Pallas kernels for 0%

profile of v1, /device:TPU:2, one launch (start us, length us, event | category | flops | bytes accessed | tf_op | source)
XLA Modules:
  0.0 552.9 jit_solution(3545508925043076282)
XLA Ops:
  7.2 0.0 copy-start
  7.2 0.0 reduce-scatter.5.cloned.1.call-start
  7.3 0.8 broadcast_multiply_fusion
  8.1 0.1 copy.37
  8.2 0.1 eq.33
  8.4 0.1 eq.29
  8.5 0.6 add_select_fusion
  9.1 0.1 copy.39
  9.2 0.2 fusion.29
  9.5 0.1 copy.36
  9.7 0.1 mul.122
  9.8 0.2 fusion.28
  10.1 2.6 scatter_custom_fusion
  12.7 0.0 copy-done.4
  12.7 0.3 fusion.4
  13.0 0.3 fusion.6
  13.3 0.1 concatenate.7
  13.4 4.1 gather_fusion
  17.5 5.4 reshape.113
  22.9 108.2 %all_to_all.10 = bf16[64,10,2048]{2,1,0:T(8,128)(2,1)S(1)} all-to-all(bf16[64,10,2048]{2,1,0:T(8,128)(2,1)} %reshape.113), channel_id=1, replica_groups=mesh['ep'=64,'tp'=4] {'ep'}, dimensions={0} | all-to-all | bytes 5242880 | tf_op jit(solution)/shard_map/all_to_all | solution.py:97
  131.1 3.0 copy.42
  134.1 0.0 copy-done.2
  134.1 1.6 collective-permute-start.1
  135.6 1.7 collective-permute-start.2
  137.3 55.4 %collective-permute-done.1 = bf16[1,64,10,2048]{3,1,2,0:T(8,128)(2,1)} collective-permute-done((bf16[1,64,10,2048]{3,1,2,0:T(8,128)(2,1)}, bf16[1,64,10,2048]{3,1,2,0:T(8,128)(2,1)}, u32[]{:S(2)}, u32[]{:S(2)}) %collective-permute-start.1) | collective-permute-done | bytes 2621472 | tf_op jit(solution)/shard_map/ppermute | solution.py:17
  192.7 0.3 collective-permute-start.3
  193.0 5.3 broadcast_in_dim.8
  198.4 2.9 copy_dynamic-update-slice_fusion
  201.3 3.6 bitcast_dynamic-update-slice_fusion.2
  204.9 0.0 collective-permute-done.2
  204.9 3.6 bitcast_dynamic-update-slice_fusion.1
  208.4 42.1 %collective-permute-done.3 = bf16[1,64,10,2048]{3,1,2,0:T(8,128)(2,1)} collective-permute-done((bf16[1,64,10,2048]{3,1,2,0:T(8,128)(2,1)}, bf16[1,64,10,2048]{3,1,2,0:T(8,128)(2,1)}, u32[]{:S(2)}, u32[]{:S(2)}) %collective-permute-start.3) | collective-permute-done | bytes 2621472 | tf_op jit(solution)/shard_map/ppermute | solution.py:17
  250.5 3.6 bitcast_dynamic-update-slice_fusion
  254.1 8.4 %fusion.14 = f32[2,256,5,256]{3,1,2,0:T(8,128)} fusion(bf16[256,2,5,2048]{3,0,2,1:T(8,128)(2,1)} %bitcast.83, bf16[2,2048,256]{2,1,0:T(8,128)(2,1)S(1)} %copy-done.12), kind=kOutput, calls=%fused_computation.25 | convolution fusion | flops 2684354560 | bytes 15204352 | tf_op jit(solution)/shard_map/nxcd,xdf->nxcf/dot_general | solution.py:111
  262.5 16.3 %convert_bitcast_fusion = bf16[256,2,5,2048]{3,0,2,1:T(8,128)(2,1)} fusion(bf16[2,256,2048]{2,1,0:T(8,128)(2,1)S(1)} %copy-done, f32[2,256,5,256]{3,1,2,0:T(8,128)} %fusion.14, bf16[256,2,5,2048]{3,0,2,1:T(8,128)(2,1)} %bitcast.84, bf16[2,2048,256]{2,1,0:T(8,128)(2,1)} %param.23), kind=kOutput, calls=%fused_computation.3 | convolution fusion | flops 5377884160 | bytes 27787264 | tf_op jit(solution)/shard_map/nxcf,xfd->nxcd/dot_general | solution.py:116
  278.8 15.3 %copy.47 = bf16[256,2,5,2048]{3,2,1,0:T(8,128)(2,1)} copy(bf16[256,2,5,2048]{3,0,2,1:T(8,128)(2,1)} %convert_bitcast_fusion) | data formatting | bytes 20971520 | tf_op jit(solution)/shard_map/convert_element_type | solution.py:118
  294.1 18.4 %convert_element_type.73 = bf16[2560,2048]{1,0:T(8,128)(2,1)} reshape(bf16[256,2,5,2048]{3,2,1,0:T(8,128)(2,1)} %copy.47) | data formatting | bytes 20971520 | tf_op jit(solution)/shard_map/convert_element_type | solution.py:118
  312.6 0.0 reduce-scatter.5.cloned.1.call-update
  312.6 0.9 copy-done.6
  313.5 2.1 collective-permute-start
  315.7 2.8 collective-permute-done
  318.5 0.1 fusion.37
  318.6 0.7 fusion.21
  319.3 0.1 broadcast_add_fusion
  319.4 0.2 copy.35
  319.6 90.7 %reduce-scatter.5.cloned.1.call-done = bf16[640,2048]{1,0:T(8,128)(2,1)} async-done(((bf16[2560,2048]{1,0:T(8,128)(2,1)}), bf16[640,2048]{1,0:T(8,128)(2,1)}) %reduce-scatter.5.cloned.1.call-update) | async-done | bytes 2621456 | tf_op jit(solution)/shard_map/reduce_scatter | solution.py:117
  410.4 5.4 reshape.114
  415.7 10.9 %all-to-all-start.1 = ((bf16[64,10,2048]{2,1,0:T(8,128)(2,1)}), bf16[64,10,2048]{2,1,0:T(8,128)(2,1)}, u32[]{:S(2)}, u32[]{:S(2)}) async-start(bf16[64,10,2048]{2,1,0:T(8,128)(2,1)} %reshape.114), calls=%async_computation.3 | async-start | bytes 8388608 | tf_op jit(solution)/shard_map/all_to_all | solution.py:125
  426.6 0.0 reduce-scatter.3.cloned.1.call-start
  426.7 0.0 copy-start.9
  426.7 2.3 convolution_convert_fusion
  429.0 0.0 reduce-scatter.3.cloned.1.call-update
  429.1 0.7 constant_dynamic-slice_fusion
  429.7 0.1 copy.48
  429.9 31.9 %reduce-scatter.3.cloned.1.call-done = bf16[128,2048]{1,0:T(8,128)(2,1)} async-done(((bf16[512,2048]{1,0:T(8,128)(2,1)}), bf16[128,2048]{1,0:T(8,128)(2,1)}) %reduce-scatter.3.cloned.1.call-update) | async-done | bytes 524304 | tf_op jit(solution)/shard_map/reduce_scatter | solution.py:101
  461.8 1.2 fusion.18
  463.0 2.0 fusion.20
  465.0 57.7 %all-to-all-done.1 = bf16[64,10,2048]{2,1,0:T(8,128)(2,1)} async-done(((bf16[64,10,2048]{2,1,0:T(8,128)(2,1)}), bf16[64,10,2048]{2,1,0:T(8,128)(2,1)}, u32[]{:S(2)}, u32[]{:S(2)}) %all-to-all-start.1) | async-done | bytes 2621472 | tf_op jit(solution)/shard_map/all_to_all | solution.py:125
  522.7 4.1 reshape.115
  526.8 3.3 gather_fusion.1
  530.1 5.4 reshape.116
  535.6 9.0 %multiply_reduce_fusion = f32[256,2048]{1,0:T(8,128)S(1)} fusion(f32[256,2,2048]{2,1,0:T(2,128)} %reshape.116, f32[256,2]{1,0:T(8,128)S(1)} %copy.48), kind=kLoop, calls=%fused_computation.4 | loop fusion | flops 1572864 | bytes 6293504 | tf_op jit(solution)/shard_map/reduce_sum | solution.py:130
  544.6 0.2 multiply_reduce_fusion.1
  544.9 1.2 multiply_convert_fusion
  (40 shorter events, 0.3 us)
Async XLA Ops:
  7.2 255.3 %copy-start = (bf16[2,256,2048]{2,1,0:T(8,128)(2,1)S(1)}, bf16[2,256,2048]{2,1,0:T(8,128)(2,1)}, u32[]{:S(2)}) copy-start(bf16[2,256,2048]{2,1,0:T(8,128)(2,1)} %param.24) | copy-start | bytes 6291460
  7.2 5.5 %copy-start.4 = (bf16[256,2048]{1,0:T(8,128)(2,1)S(1)}, bf16[256,2048]{1,0:T(8,128)(2,1)}, u32[]{:S(2)}) copy-start(bf16[256,2048]{1,0:T(8,128)(2,1)} %param.18) | copy-start | bytes 3145732
  7.2 5.8 %copy-start.8 = (f32[2048]{0:T(1024)S(1)}, f32[2048]{0:T(1024)}, u32[]{:S(2)}) copy-start(f32[2048]{0:T(1024)} %param.21) | copy-start | bytes 24580
  7.2 403.2 %reduce-scatter.5.cloned.1.call-start = ((), (), s32[]{:S(2)}) async-start(), calls=%async_computation.5 | async-start | bytes 13107200 | tf_op jit(solution)/shard_map/reduce_scatter | solution.py:117
  131.1 3.0 copy-start.2
  134.1 58.7 %collective-permute-start.1 = (bf16[1,64,10,2048]{3,1,2,0:T(8,128)(2,1)}, bf16[1,64,10,2048]{3,1,2,0:T(8,128)(2,1)}, u32[]{:S(2)}, u32[]{:S(2)}) collective-permute-start(bf16[1,64,10,2048]{3,1,2,0:T(8,128)(2,1)} %copy.42), channel_id=1, source_target_pairs={{0,1},{1,2},{2,3},{3,0},{4,5},{5,6},{6,7},{7,4},{8,9},{9,10},{10,1... | collective-permute-start | bytes 7864328 | tf_op jit(solution)/shard_map/ppermute | solution.py:17
  135.6 69.2 %collective-permute-start.2 = (bf16[1,64,10,2048]{3,1,2,0:T(8,128)(2,1)}, bf16[1,64,10,2048]{3,1,2,0:T(8,128)(2,1)}, u32[]{:S(2)}, u32[]{:S(2)}) collective-permute-start(bf16[1,64,10,2048]{3,1,2,0:T(8,128)(2,1)} %copy.42), channel_id=1, source_target_pairs={{0,3},{1,0},{2,1},{3,2},{4,7},{5,4},{6,5},{7,6},{8,11},{9,8},{10,9... | collective-permute-start | bytes 7864328 | tf_op jit(solution)/shard_map/ppermute | solution.py:20
  192.7 57.8 %collective-permute-start.3 = (bf16[1,64,10,2048]{3,1,2,0:T(8,128)(2,1)}, bf16[1,64,10,2048]{3,1,2,0:T(8,128)(2,1)}, u32[]{:S(2)}, u32[]{:S(2)}) collective-permute-start(bf16[1,64,10,2048]{3,1,2,0:T(8,128)(2,1)} %collective-permute-done.1), channel_id=1, source_target_pairs={{0,1},{1,2},{2,3},{3,0},{4,5},{5,6},{6,7},{7,4},{8,9},{9,10},{10,1... | collective-permute-start | bytes 7864328 | tf_op jit(solution)/shard_map/ppermute | solution.py:17
  193.0 5.3 copy-start.3
  208.4 45.7 %copy-start.12 = (bf16[2,2048,256]{2,1,0:T(8,128)(2,1)S(1)}, bf16[2,2048,256]{2,1,0:T(8,128)(2,1)}, u32[]{:S(2)}) copy-start(bf16[2,2048,256]{2,1,0:T(8,128)(2,1)} %param.22) | copy-start | bytes 6291460
  312.6 0.9 copy-start.6
  313.5 5.0 collective-permute-start
  415.7 11.0 %copy-start.5 = (bf16[256,2048]{1,0:T(8,128)(2,1)S(1)}, bf16[256,2048]{1,0:T(8,128)(2,1)}, u32[]{:S(2)}) copy-start(bf16[256,2048]{1,0:T(8,128)(2,1)} %param.16) | copy-start | bytes 3145732
  415.7 11.0 %copy-start.7 = (bf16[1,256,256]{2,1,0:T(8,128)(2,1)S(1)}, bf16[1,256,256]{2,1,0:T(8,128)(2,1)}, u32[]{:S(2)}) copy-start(bf16[1,256,256]{2,1,0:T(8,128)(2,1)} %param.14) | copy-start | bytes 393220
  415.7 11.0 %copy-start.11 = (f32[256]{0:T(256)S(1)}, f32[256]{0:T(256)}, u32[]{:S(2)}) copy-start(f32[256]{0:T(256)} %param.15) | copy-start | bytes 3076
  415.7 107.0 %all-to-all-start.1 = ((bf16[64,10,2048]{2,1,0:T(8,128)(2,1)}), bf16[64,10,2048]{2,1,0:T(8,128)(2,1)}, u32[]{:S(2)}, u32[]{:S(2)}) async-start(bf16[64,10,2048]{2,1,0:T(8,128)(2,1)} %reshape.114), calls=%async_computation.3 | async-start | bytes 8388608 | tf_op jit(solution)/shard_map/all_to_all | solution.py:125
  426.6 35.1 %reduce-scatter.3.cloned.1.call-start = ((), (), s32[]{:S(2)}) async-start(), calls=%async_computation.4 | async-start | bytes 2621440 | tf_op jit(solution)/shard_map/reduce_scatter | solution.py:101
  426.7 36.3 %copy-start.9 = (f32[2048]{0:T(1024)S(1)}, f32[2048]{0:T(1024)}, u32[]{:S(2)}) copy-start(f32[2048]{0:T(1024)} %param.17) | copy-start | bytes 24580
  535.6 9.3 %copy-start.10 = (f32[2048]{0:T(1024)S(1)}, f32[2048]{0:T(1024)}, u32[]{:S(2)}) copy-start(f32[2048]{0:T(1024)} %param.25) | copy-start | bytes 24580
  535.6 10.5 %copy-start.1 = (bf16[2,256,2048]{2,1,0:T(8,128)(2,1)S(1)}, bf16[2,256,2048]{2,1,0:T(8,128)(2,1)}, u32[]{:S(2)}) copy-start(bf16[2,256,2048]{2,1,0:T(8,128)(2,1)} %param.24) | copy-start | bytes 6291460
Sparse Core Ops, SparseCore 0:
  312.7 97.6 reduce-scatter.4
  430.0 31.7 reduce-scatter.2
